TPU v7x, 32 devices: a whole 2x2x4 slice. The times are simulated.
32 devices in a mesh: rep: 2 (over x), fs: 4 (over z), tp: 4 (over y, core).
Axes of the slice: x: 2, y: 2, z: 4, core: 2. Of those that a mesh axis runs over, the one named last changes fastest.
Arguments:
- tokens: bfloat16 [8192, 1024], P(('rep', 'fs', 'tp')), may hold values from -6 to 6
- norm_gain: float32 [1024], replicated, may hold values from 0.5 to 1.5
- gate_weight: bfloat16 [1024, 3072], P(('rep', 'fs'), 'tp'), may hold values from -0.1875 to 0.1875
- up_weight: bfloat16 [1024, 3072], P(('rep', 'fs'), 'tp'), may hold values from -0.1875 to 0.1875
- down_weight: bfloat16 [3072, 1024], P('tp', ('rep', 'fs')), may hold values from -0.109375 to 0.109375
Outputs:
- block_out: bfloat16 [8192, 1024], P(('rep', 'fs', 'tp'))
All inputs are finite; a program needn't handle non-finite values.
Results may differ from a plain program's by a relative error of at most 0.001.
Values may be sent and summed in bfloat16 or wider, within the bound.
A program may use at most 64 MiB of HBM per device.

v0:
```python
import jax
import jax.numpy as jnp
from jax import lax
from jax.sharding import PartitionSpec as P

epsilon = 1e-06


def over_all(shard, axis, dim, absorb, carry):
    whole = jax.tree.map(lambda part: lax.all_gather(part, axis, axis=dim, tiled=True), shard)
    return absorb(carry, whole, jnp.int32(0))


def summed_rows(portion, width, axis):
    count = width * lax.axis_size(axis)
    return lax.psum_scatter(portion(jnp.int32(0), count), axis, scatter_dimension=0, tiled=True)


def on_device(tokens, norm_gain, gate_weight, up_weight, down_weight):
    values = tokens.astype(jnp.float32)
    inverse_rms = lax.rsqrt(jnp.mean(values * values, axis=-1, keepdims=True) + epsilon)
    normed = (values * inverse_rms * norm_gain.astype(jnp.float32)).astype(jnp.bfloat16)
    gathered = lax.all_gather(normed, "tp", axis=0, tiled=True)
    zero_sums = jnp.zeros((gathered.shape[0], gate_weight.shape[1]), jnp.float32)

    def add_block(running, row_block, first_row):
        columns = lax.dynamic_slice_in_dim(gathered, first_row, row_block.shape[0], 1)
        return running + jnp.dot(columns, row_block, preferred_element_type=jnp.float32)

    gate_value = over_all(gate_weight, ("rep", "fs"), 0, add_block, zero_sums)
    up_value = over_all(up_weight, ("rep", "fs"), 0, add_block, zero_sums)
    hidden = (jax.nn.silu(gate_value) * up_value).astype(jnp.bfloat16)
    own_half = lax.all_gather(down_weight, "fs", axis=1, tiled=True)
    down_whole = lax.all_gather(own_half, "rep", axis=1, tiled=True)
    own_rows = tokens.shape[0]

    def row_terms(first_row, row_count):
        token_block = lax.dynamic_slice_in_dim(hidden, first_row, row_count, 0)
        return jnp.dot(token_block, down_whole, preferred_element_type=jnp.float32)

    mixed_out = summed_rows(row_terms, own_rows, "tp")
    return mixed_out.astype(jnp.bfloat16)


def solution(mesh):
    return jax.shard_map(
        on_device,
        mesh=mesh,
        in_specs=(
            P(("rep", "fs", "tp"), None),
            P(),
            P(("rep", "fs"), "tp"),
            P(("rep", "fs"), "tp"),
            P("tp", ("rep", "fs")),
        ),
        out_specs=P(("rep", "fs", "tp"), None),
        check_vma=False,
    )
```

profile of v0, /device:TPU:0, one launch (start us, length us, event | category | flops | bytes accessed | tf_op | source)
XLA Modules:
  0.0 218.2 jit_solution(9125715528160293608)
XLA Ops:
  6.5 0.0 copy-start
  6.5 0.0 all-gather.7.cloned.1.call-start
  6.5 0.7 all-gather.7.cloned.1.call-update
  7.3 0.0 all-gather.5.cloned.1.call-start
  7.3 1.2 fusion.1
  8.5 2.0 fusion.3
  10.6 0.0 all-gather.5.cloned.1.call-update
  10.6 0.0 all-gather.11.cloned.1.call-start
  10.6 0.0 copy-done
  10.7 26.2 %all_gather.18 = bf16[768,512]{1,0:T(8,128)(2,1)} all-gather(bf16[768,128]{1,0:T(8,128)(2,1)S(1)} %copy-done), channel_id=1, replica_groups=mesh['rep'=2,'fs'=4,'tp'=4] {'fs'}, dimensions={1}, use_global_device_ids=true | all-gather | bytes 983040 | tf_op jit(solution)/shard_map/all_gather | solution.py:33
  36.8 0.0 all-gather.11.cloned.1.call-update
  36.9 0.0 all-gather.9.cloned.1.call-start
  36.9 0.5 all-gather.9.cloned.1.call-update
  37.5 0.0 reduce-scatter.2.cloned.1.call-start
  37.5 22.4 %all-gather.7.cloned.1.call-done = bf16[1024,768]{1,0:T(8,128)(2,1)} async-done(((bf16[128,768]{1,0:T(8,128)(2,1)}), bf16[1024,768]{1,0:T(8,128)(2,1)}) %all-gather.7.cloned.1.call-update) | async-done | bytes 1572880 | tf_op jit(solution)/shard_map/all_gather | solution.py:10
  59.9 22.5 %all-gather.5.cloned.1.call-done = bf16[1024,1024]{1,0:T(8,128)(2,1)} async-done(((bf16[256,1024]{1,0:T(8,128)(2,1)}), bf16[1024,1024]{1,0:T(8,128)(2,1)}) %all-gather.5.cloned.1.call-update) | async-done | bytes 2097168 | tf_op jit(solution)/shard_map/all_gather | solution.py:23
  82.4 0.0 copy-start.1
  82.4 5.6 %fusion.5 = f32[1024,768]{1,0:T(8,128)} fusion(bf16[1024,1024]{1,0:T(8,128)(2,1)} %all-gather.5.cloned.1.call-done, bf16[1024,768]{1,0:T(8,128)(2,1)} %all-gather.7.cloned.1.call-done), kind=kOutput, calls=%fused_computation.9 | convolution fusion | flops 1610612736 | bytes 6815744 | tf_op jit(solution)/shard_map/dot_general | solution.py:28
  88.0 23.1 %all-gather.11.cloned.1.call-done = bf16[768,1024]{1,0:T(8,128)(2,1)} async-done(((bf16[768,512]{1,0:T(8,128)(2,1)}), bf16[768,1024]{1,0:T(8,128)(2,1)}) %all-gather.11.cloned.1.call-update) | async-done | bytes 1572880 | tf_op jit(solution)/shard_map/all_gather | solution.py:34
  111.2 46.2 %all-gather.9.cloned.1.call-done = bf16[1024,768]{1,0:T(8,128)(2,1)} async-done(((bf16[128,768]{1,0:T(8,128)(2,1)}), bf16[1024,768]{1,0:T(8,128)(2,1)}) %all-gather.9.cloned.1.call-update) | async-done | bytes 1572880 | tf_op jit(solution)/shard_map/all_gather | solution.py:10
  157.3 0.0 copy-done.1
  157.3 9.1 %fusion = f32[1024,1024]{1,0:T(8,128)} fusion(bf16[768,1024]{1,0:T(8,128)(2,1)} %all-gather.11.cloned.1.call-done, f32[1024,768]{1,0:T(8,128)} %fusion.5, bf16[1024,1024]{1,0:T(8,128)(2,1)S(1)} %copy-done.1, bf16[1024,768]{1,0:T(8,128)(2,1)} %all-gather.9.cloned.1.call-done), kind=kOutput, calls=%fused_computation.1 | convolution fusion | flops 3225944064 | bytes 12582912 | tf_op jit(solution)/shard_map/dot_general | solution.py:39
  166.5 0.0 reduce-scatter.2.cloned.1.call-update
  166.5 43.1 %reduce-scatter.2.cloned.1.call-done = f32[256,1024]{1,0:T(8,128)} async-done(((f32[1024,1024]{1,0:T(8,128)}), f32[256,1024]{1,0:T(8,128)}) %reduce-scatter.2.cloned.1.call-update) | async-done | bytes 1048592 | tf_op jit(solution)/shard_map/reduce_scatter | solution.py:16
  209.6 2.1 convert_element_type.15
  (1 shorter events, 0.0 us)
Async XLA Ops:
  6.5 4.1 %copy-start = (bf16[768,128]{1,0:T(8,128)(2,1)S(1)}, bf16[768,128]{1,0:T(8,128)(2,1)}, u32[]{:S(2)}) copy-start(bf16[768,128]{1,0:T(8,128)(2,1)} %param.9) | copy-start | bytes 589828
  6.5 53.3 %all-gather.7.cloned.1.call-start = ((), (), s32[]{:S(2)}) async-start(), calls=%async_computation.2 | async-start | bytes 1769472 | tf_op jit(solution)/shard_map/all_gather | solution.py:10
  7.3 75.1 %all-gather.5.cloned.1.call-start = ((), (), s32[]{:S(2)}) async-start(), calls=%async_computation.1 | async-start | bytes 2621440 | tf_op jit(solution)/shard_map/all_gather | solution.py:23
  10.6 100.6 %all-gather.11.cloned.1.call-start = ((), (), s32[]{:S(2)}) async-start(), calls=%async_computation.4 | async-start | bytes 2359296 | tf_op jit(solution)/shard_map/all_gather | solution.py:34
  36.9 120.5 %all-gather.9.cloned.1.call-start = ((), (), s32[]{:S(2)}) async-start(), calls=%async_computation.3 | async-start | bytes 1769472 | tf_op jit(solution)/shard_map/all_gather | solution.py:10
  37.5 172.1 %reduce-scatter.2.cloned.1.call-start = ((), (), s32[]{:S(2)}) async-start(), calls=%async_computation.5 | async-start | bytes 5242880 | tf_op jit(solution)/shard_map/reduce_scatter | solution.py:16
  82.4 74.9 %copy-start.1 = (bf16[1024,1024]{1,0:T(8,128)(2,1)S(1)}, bf16[1024,1024]{1,0:T(8,128)(2,1)}, u32[]{:S(2)}) copy-start(bf16[1024,1024]{1,0:T(8,128)(2,1)} %all-gather.5.cloned.1.call-done) | copy-start | bytes 6291460
Sparse Core Ops, SparseCore 0:
  9.4 50.3 all-gather.6
  61.4 20.9 all-gather.4
  83.9 27.1 all-gather.10
  113.1 44.1 all-gather.8
  166.6 42.9 reduce-scatter.1
where the time goes:
time: 218 us
  waiting for transfers between devices  159 us (73%)
  blocking collectives  26.2 us (12%)
  matrix products  14.8 us (7%)
  between operations  13.2 us (6%)
  other arithmetic  5.36 us (2%)
    all_gather x2, waiting for transfers between devices, over_all(): lax.all_gather(part, axis, axis=dim, tiled=True)  68.5 us
    reduce_scatter x1, waiting for transfers between devices, summed_rows(): lax.psum_scatter(portion(jnp.int32(0), count), axis, scatter_dimension=0,...  43.1 us
    all_gather x1, blocking collectives, on_device(): own_half = lax.all_gather(down_weight, 'fs', axis=1, tiled=True)  26.2 us
    all_gather x1, waiting for transfers between devices, on_device(): down_whole = lax.all_gather(own_half, 'rep', axis=1, tiled=True)  23.1 us
    all_gather x1, waiting for transfers between devices, on_device(): gathered = lax.all_gather(normed, 'tp', axis=0, tiled=True)  22.5 us
    dot_general x1, matrix products, row_terms(): return jnp.dot(token_block, down_whole, preferred_element_type=jnp.float32)  9.14 us
    dot_general x1, matrix products, add_block(): jnp.dot(columns, row_block, preferred_element_type=jnp.float32)  5.65 us
  transfers between devices with their start and end apart: 5, of which 5 were waited for; matrix products, arithmetic and copies ran while one was open for 4% of the time, Pallas kernels for 0%

commit v1 on v0

--- a/solution.py
+++ b/solution.py
@@ -31,7 +31,7 @@
     up_value = over_all(up_weight, ("rep", "fs"), 0, add_block, zero_sums)
     hidden = (jax.nn.silu(gate_value) * up_value).astype(jnp.bfloat16)
     own_half = lax.all_gather(down_weight, "fs", axis=1, tiled=True)
-    down_whole = lax.all_gather(own_half, "rep", axis=1, tiled=True)
+    down_whole = jnp.concatenate(lax.all_gather(own_half, "rep"), 1)
     own_rows = tokens.shape[0]
 
     def row_terms(first_row, row_count):

time: 218 us -> 230 us (1.055)
  waiting for transfers between devices: 159 us -> 176 us
  blocking collectives: 26.2 us -> 21.2 us
    all_gather x2, waiting for transfers between devices: 68.5 us -> 85.3 us  [over_all(): lax.all_gather(part, axis, axis=dim, tiled=True)]
    all_gather x1, blocking collectives: 26.2 us -> 21.2 us  [on_device(): own_half = lax.all_gather(down_weight, 'fs', axis=1, tiled=True)]
where the time goes in v1:
time: 230 us
  waiting for transfers between devices  176 us (77%)
  blocking collectives  21.2 us (9%)
  matrix products  14.8 us (6%)
  between operations  13.2 us (6%)
  other arithmetic  3.27 us (1%)
    all_gather x2, waiting for transfers between devices, over_all(): lax.all_gather(part, axis, axis=dim, tiled=True)  85.3 us
    reduce_scatter x1, waiting for transfers between devices, summed_rows(): lax.psum_scatter(portion(jnp.int32(0), count), axis, scatter_dimension=0,...  43.1 us
    all_gather x1, waiting for transfers between devices, on_device(): down_whole = jnp.concatenate(lax.all_gather(own_half, 'rep'), 1)  23.8 us
    all_gather x1, waiting for transfers between devices, on_device(): gathered = lax.all_gather(normed, 'tp', axis=0, tiled=True)  22.5 us
    all_gather x1, blocking collectives, on_device(): own_half = lax.all_gather(down_weight, 'fs', axis=1, tiled=True)  21.2 us
    dot_general x1, matrix products, row_terms(): return jnp.dot(token_block, down_whole, preferred_element_type=jnp.float32)  9.31 us
    dot_general x1, matrix products, add_block(): jnp.dot(columns, row_block, preferred_element_type=jnp.float32)  5.5 us
  transfers between devices with their start and end apart: 5, of which 5 were waited for; matrix products, arithmetic and copies ran while one was open for 4% of the time, Pallas kernels for 0%

profile of v1, /device:TPU:0, one launch (start us, length us, event | category | flops | bytes accessed | tf_op | source)
XLA Modules:
  0.0 230.3 jit_solution(12556468927730539275)
XLA Ops:
  6.5 0.0 copy-start
  6.5 0.0 copy-start.1
  6.5 0.0 all-gather.12.cloned.1.call-start
  6.5 21.2 %all_gather.21 = bf16[768,512]{1,0:T(8,128)(2,1)} all-gather(bf16[768,128]{1,0:T(8,128)(2,1)} %param.9), channel_id=1, replica_groups=mesh['rep'=2,'fs'=4,'tp'=4] {'fs'}, dimensions={1}, use_global_device_ids=true | all-gather | bytes 983040 | tf_op jit(solution)/shard_map/all_gather | solution.py:33
  27.7 0.0 all-gather.12.cloned.1.call-update
  27.8 0.0 all-gather.8.cloned.1.call-start
  27.8 0.7 all-gather.8.cloned.1.call-update
  28.5 0.0 all-gather.6.cloned.1.call-start
  28.6 0.0 copy-done
  28.6 0.2 fusion.1
  28.8 0.0 copy-done.1
  28.8 1.0 fusion.3
  29.7 0.0 all-gather.6.cloned.1.call-update
  29.8 0.0 all-gather.10.cloned.1.call-start
  29.8 0.5 all-gather.10.cloned.1.call-update
  30.3 0.0 reduce-scatter.2.cloned.1.call-start
  30.4 23.8 %all-gather.12.cloned.1.call-done = bf16[1536,512]{1,0:T(8,128)(2,1)} async-done(((bf16[768,512]{1,0:T(8,128)(2,1)}), bf16[1536,512]{1,0:T(8,128)(2,1)}) %all-gather.12.cloned.1.call-update) | async-done | bytes 1572880 | tf_op jit(solution)/shard_map/all_gather | solution.py:34
  54.2 1.7 copy.6
  55.9 44.6 %all-gather.8.cloned.1.call-done = bf16[1024,768]{1,0:T(8,128)(2,1)} async-done(((bf16[128,768]{1,0:T(8,128)(2,1)}), bf16[1024,768]{1,0:T(8,128)(2,1)}) %all-gather.8.cloned.1.call-update) | async-done | bytes 1572880 | tf_op jit(solution)/shard_map/all_gather | solution.py:10
  100.5 22.5 %all-gather.6.cloned.1.call-done = bf16[1024,1024]{1,0:T(8,128)(2,1)} async-done(((bf16[256,1024]{1,0:T(8,128)(2,1)}), bf16[1024,1024]{1,0:T(8,128)(2,1)}) %all-gather.6.cloned.1.call-update) | async-done | bytes 2097168 | tf_op jit(solution)/shard_map/all_gather | solution.py:23
  123.0 5.5 %fusion.5 = f32[1024,768]{1,0:T(8,128)} fusion(bf16[1024,1024]{1,0:T(8,128)(2,1)} %all-gather.6.cloned.1.call-done, bf16[1024,768]{1,0:T(8,128)(2,1)} %all-gather.8.cloned.1.call-done), kind=kOutput, calls=%fused_computation.9 | convolution fusion | flops 1610612736 | bytes 6815744 | tf_op jit(solution)/shard_map/dot_general | solution.py:28
  128.5 40.7 %all-gather.10.cloned.1.call-done = bf16[1024,768]{1,0:T(8,128)(2,1)} async-done(((bf16[128,768]{1,0:T(8,128)(2,1)}), bf16[1024,768]{1,0:T(8,128)(2,1)}) %all-gather.10.cloned.1.call-update) | async-done | bytes 1572880 | tf_op jit(solution)/shard_map/all_gather | solution.py:10
  169.2 9.3 %fusion = f32[1024,1024]{1,0:T(8,128)} fusion(bf16[768,1024]{0,1:T(8,128)(2,1)S(1)} %bitcast.10, f32[1024,768]{1,0:T(8,128)} %fusion.5, bf16[1024,1024]{1,0:T(8,128)(2,1)} %all-gather.6.cloned.1.call-done, bf16[1024,768]{1,0:T(8,128)(2,1)} %all-gather.10.cloned.1.call-done), kind=kOutput, calls=%fused_computation.1 | convolution fusion | flops 3225944064 | bytes 12582912 | tf_op jit(solution)/shard_map/dot_general | solution.py:39
  178.5 0.0 reduce-scatter.2.cloned.1.call-update
  178.6 43.1 %reduce-scatter.2.cloned.1.call-done = f32[256,1024]{1,0:T(8,128)} async-done(((f32[1024,1024]{1,0:T(8,128)}), f32[256,1024]{1,0:T(8,128)}) %reduce-scatter.2.cloned.1.call-update) | async-done | bytes 1048592 | tf_op jit(solution)/shard_map/reduce_scatter | solution.py:16
  221.7 2.1 convert_element_type.15
  (1 shorter events, 0.0 us)
Async XLA Ops:
  6.5 22.0 %copy-start = (bf16[256,1024]{1,0:T(8,128)(2,1)S(1)}, bf16[256,1024]{1,0:T(8,128)(2,1)}, u32[]{:S(2)}) copy-start(bf16[256,1024]{1,0:T(8,128)(2,1)} %param.5) | copy-start | bytes 1572868
  6.5 22.2 %copy-start.1 = (f32[1024]{0:T(1024)S(1)}, f32[1024]{0:T(1024)}, u32[]{:S(2)}) copy-start(f32[1024]{0:T(1024)} %param.6) | copy-start | bytes 12292
  6.5 47.6 %all-gather.12.cloned.1.call-start = ((), (), s32[]{:S(2)}) async-start(), calls=%async_computation.5 | async-start | bytes 2359296 | tf_op jit(solution)/shard_map/all_gather | solution.py:34
  27.8 72.8 %all-gather.8.cloned.1.call-start = ((), (), s32[]{:S(2)}) async-start(), calls=%async_computation.2 | async-start | bytes 1769472 | tf_op jit(solution)/shard_map/all_gather | solution.py:10
  28.5 94.5 %all-gather.6.cloned.1.call-start = ((), (), s32[]{:S(2)}) async-start(), calls=%async_computation.1 | async-start | bytes 2621440 | tf_op jit(solution)/shard_map/all_gather | solution.py:23
  29.8 139.4 %all-gather.10.cloned.1.call-start = ((), (), s32[]{:S(2)}) async-start(), calls=%async_computation.3 | async-start | bytes 1769472 | tf_op jit(solution)/shard_map/all_gather | solution.py:10
  30.3 191.3 %reduce-scatter.2.cloned.1.call-start = ((), (), s32[]{:S(2)}) async-start(), calls=%async_computation.4 | async-start | bytes 5242880 | tf_op jit(solution)/shard_map/reduce_scatter | solution.py:16
Sparse Core Ops, SparseCore 0:
  27.9 26.2 all-gather.11
  56.3 44.1 all-gather.7
  102.1 20.9 all-gather.5
  125.0 44.1 all-gather.9
  178.7 42.9 reduce-scatter.1
